TPU v7x, 256 devices: a 4x2x16 block of a 4x16x16 slice. The times are simulated.
256 devices in a mesh: grp: 2 (over y), ep: 64 (over z, x), tp: 2 (over core).
Axes of the slice: x: 4, y: 2, z: 16, core: 2. Of those that a mesh axis runs over, the one named last changes fastest.
The devices are a block of a 4x16x16 slice.
Arguments:
- tokens: bfloat16 [16384, 2048], P(('grp', 'ep')), parts along dimension 0, may hold values from -6 to 6
- in_gain: float32 [2048], replicated, may hold values from 0.1 to 1.9
- routing: int32 [16384, 4], P(('grp', 'ep')), parts along dimension 0, may hold values from 0 to 127, as said below
- gate_prob: float32 [16384, 4], P(('grp', 'ep')), parts along dimension 0, may hold values from 0.05 to 1
- w_gate: bfloat16 [128, 2048, 512], P('ep', None, 'tp'), may hold values from -0.125 to 0.125
- w_up: bfloat16 [128, 2048, 512], P('ep', None, 'tp'), may hold values from -0.125 to 0.125
- w_down: bfloat16 [128, 512, 2048], P('ep', 'tp')
- out_gain: float32 [2048], P('tp'), may hold values from 0.1 to 1.9
Outputs:
- output: bfloat16 [16384, 2048], P(('grp', 'ep'), 'tp'), parts along dimension 0
There are 2 independent parts, one for each index of `grp`. A program takes and returns all parts, laid end to end along the dimension named above; an argument that names none is the same for every part. Nothing has to cross between parts.
Inputs may be any that keep to these rules, and one draw needn't show every extreme that they name: `routing`: each row names 4 different experts, all of one group (the same value of expert // 32). In the rows of one device no expert is named more than 8 times, and in every device's rows some expert is named exactly 8 times.
All inputs are finite; a program needn't handle non-finite values.
Results may differ from a plain program's by a relative error of at most 0.0077.
Values may be sent and summed in bfloat16 or wider, within the bound.
A program may use at most 64 MiB of HBM per device.

v0:
```python
import jax
import jax.numpy as jnp
from jax import lax
from jax.sharding import PartitionSpec as P

GROUPS = 4
EPS = 1e-06


def split_up(value, dim, peers):
    dims = value.shape
    tiles = value.reshape(*dims[:dim], peers, dims[dim] // peers, *dims[dim + 1 :])
    return jnp.moveaxis(tiles, dim, 0)


def sent_and_summed(value, axis, dim):
    tiles = split_up(value, dim, lax.axis_size(axis))
    arrived = lax.all_to_all(tiles, axis, split_axis=0, concat_axis=0, tiled=True)
    return arrived.astype(jnp.float32).sum(axis=0)


def gathered_total(value, axis):
    tiles = lax.all_gather(value, axis)
    return tiles.sum(axis=0)


def slot_ranks(flat_routes, expert_count):
    matches = (flat_routes[:, None] == jnp.arange(expert_count, dtype=jnp.int32)[None, :]).astype(
        jnp.int32
    )
    earlier = jnp.cumsum(matches, axis=0) - matches
    return jnp.sum(earlier * matches, axis=1)


def fill_rows(source, entries):
    filled = entries > 0
    return jnp.where(
        filled[:, None], source[jnp.maximum(entries - 1, 0)], jnp.zeros((), source.dtype)
    )


def body(tokens, in_gain, routing, gate_prob, w_gate, w_up, w_down, out_gain):
    ep_count = lax.axis_size("ep")
    local_experts = w_gate.shape[0]
    expert_count = local_experts * ep_count
    tok_dev, top_count = routing.shape
    model_width = tokens.shape[1]
    half_width = out_gain.shape[0]
    group_width = expert_count // GROUPS
    row_cap = max(2, tok_dev * top_count // (2 * group_width))
    floats = tokens.astype(jnp.float32)
    normed = (
        floats * lax.rsqrt(jnp.mean(floats * floats, axis=-1, keepdims=True) + EPS) * in_gain
    ).astype(jnp.bfloat16)
    flat_routes = routing.reshape(-1)
    slot_rank = slot_ranks(flat_routes, expert_count)
    slot_ids = flat_routes * row_cap + slot_rank
    token_ids = jnp.arange(tok_dev * top_count, dtype=jnp.int32) // top_count
    slot_table = jnp.zeros((expert_count * row_cap,), jnp.int32).at[slot_ids].set(token_ids + 1)
    own_columns = lax.dynamic_slice_in_dim(normed, lax.axis_index("tp") * half_width, half_width, 1)
    sendbuf = fill_rows(own_columns, slot_table).reshape(
        ep_count, local_experts, row_cap, half_width
    )
    arrived = lax.all_to_all(sendbuf, "ep", split_axis=0, concat_axis=0, tiled=True)
    arrived = lax.all_gather(arrived, "tp", axis=3, tiled=True)
    gate_act = jnp.einsum("secd,edf->secf", arrived, w_gate, preferred_element_type=jnp.float32)
    up_act = jnp.einsum("secd,edf->secf", arrived, w_up, preferred_element_type=jnp.float32)
    hidden = (jax.nn.silu(gate_act) * up_act).astype(jnp.bfloat16)
    partial_out = jnp.einsum("secf,efd->secd", hidden, w_down, preferred_element_type=jnp.float32)
    results = sent_and_summed(partial_out.astype(jnp.bfloat16), "tp", 3).astype(jnp.bfloat16)
    returned = lax.all_to_all(results, "ep", split_axis=0, concat_axis=0, tiled=True).reshape(
        expert_count * row_cap, half_width
    )
    picked = returned[slot_ids].astype(jnp.float32).reshape(tok_dev, top_count, half_width)
    mixed_rows = jnp.sum(picked * gate_prob[:, :, None], axis=1)
    squares = jnp.sum(mixed_rows * mixed_rows, axis=1)
    total_squares = gathered_total(squares, "tp")
    inv_rms = lax.rsqrt(total_squares / model_width + EPS)
    return (mixed_rows * inv_rms[:, None] * out_gain).astype(jnp.bfloat16)


def solution(mesh):
    placed = (
        P(("grp", "ep"), None),
        P(),
        P(("grp", "ep"), None),
        P(("grp", "ep"), None),
        P("ep", None, "tp"),
        P("ep", None, "tp"),
        P("ep", "tp", None),
        P("tp"),
    )
    return jax.shard_map(
        body, mesh=mesh, in_specs=placed, out_specs=P(("grp", "ep"), "tp"), check_vma=False
    )
```

profile of v0, /device:TPU:33, one launch (start us, length us, event | category | flops | bytes accessed | tf_op | source)
XLA Modules:
  0.0 331.5 jit_solution(8232878903041759823)
XLA Ops:
  6.6 1.3 convert_element_type.36
  7.9 1.2 multiply_reduce_fusion.1
  9.1 0.1 copy.29
  9.3 0.1 eq.25
  9.4 0.1 copy.31
  9.6 0.2 fusion.24
  9.9 0.1 copy.28
  10.0 0.1 mul.77
  10.1 0.2 fusion.23
  10.3 2.4 scatter_custom_fusion
  12.8 0.1 broadcast_in_dim.16
  13.0 0.1 fusion.20
  13.1 5.4 %gather_fusion = bf16[1024,1024]{1,0:T(8,128)(2,1)} fusion(bf16[128,1024]{1,0:T(8,128)(2,1)S(1)} %fusion.20, s32[1024]{0:T(1024)S(1)} %maximum_clamp_fusion), kind=kCustom, calls=%fused_computation | custom fusion | bytes 4198400 | tf_op jit(solution)/shard_map/gather | solution.py:38
  18.5 1.8 broadcast_select_fusion
  20.3 124.6 %all_to_all.15 = bf16[64,2,8,1024]{3,2,1,0:T(8,128)(2,1)S(1)} all-to-all(bf16[64,2,8,1024]{3,2,1,0:T(8,128)(2,1)S(1)} %broadcast_select_fusion), channel_id=1, replica_groups=mesh['grp'=2,'ep'=64,'tp'=2] {'ep'}, dimensions={0} | all-to-all | bytes 4194304 | tf_op jit(solution)/shard_map/all_to_all | solution.py:64
  144.9 1.5 copy.33
  146.5 19.9 %all-gather.4.cloned.1.call-done = bf16[64,2,8,2048]{3,2,0,1:T(8,128)(2,1)} async-done(((bf16[64,2,8,1024]{3,2,0,1:T(8,128)(2,1)}), bf16[64,2,8,2048]{3,2,0,1:T(8,128)(2,1)}) %all-gather.4.cloned.1.call-update) | async-done | bytes 4194320 | tf_op jit(solution)/shard_map/all_gather | solution.py:65
  166.4 4.1 %fusion.5 = f32[64,2,8,256]{3,2,0,1:T(8,128)S(1)} fusion(bf16[64,2,8,2048]{3,2,0,1:T(8,128)(2,1)} %all-gather.4.cloned.1.call-done, bf16[2,2048,256]{2,1,0:T(8,128)(2,1)} %param.12), kind=kOutput, calls=%fused_computation.12 | convolution fusion | flops 1073741824 | bytes 7340032 | tf_op jit(solution)/shard_map/secd,edf->secf/dot_general | solution.py:66
  170.5 7.2 %convolution_convert_fusion = bf16[2,64,8,2048]{3,2,1,0:T(8,128)(2,1)} fusion(bf16[2,256,2048]{2,1,0:T(8,128)(2,1)S(1)} %copy-done, bf16[64,2,8,2048]{3,2,0,1:T(8,128)(2,1)} %all-gather.4.cloned.1.call-done, bf16[2,2048,256]{2,1,0:T(8,128)(2,1)} %param.13, f32[64,2,8,256]{3,2,0,1:T(8,128)S(1)} %fusion.5), kind=kOutput, calls=%fused_computation.4 | convolution fusion | flops 2151153664 | bytes 13631488 | tf_op jit(solution)/shard_map/secf,efd->secd/dot_general | solution.py:69
  177.7 2.6 copy.43
  180.4 8.0 %all_to_all.16 = bf16[2,64,2,8,1024]{4,3,1,2,0:T(8,128)(2,1)} all-to-all(bf16[2,64,2,8,1024]{4,3,1,2,0:T(8,128)(2,1)S(1)} %bitcast.61), channel_id=1, replica_groups=mesh['grp'=2,'ep'=64,'tp'=2] {'tp'}, dimensions={0} | all-to-all | bytes 8388608 | tf_op jit(solution)/shard_map/all_to_all | solution.py:18
  188.4 5.2 %reduce_sum.62 = bf16[64,2,8,1024]{3,2,0,1:T(8,128)(2,1)} reduce(bf16[2,64,2,8,1024]{4,3,1,2,0:T(8,128)(2,1)} %all_to_all.16, bf16[]{:T(256)} %constant.55.clone.1), dimensions={0}, to_apply=%region_5.6 | reduce | flops 1048576 | bytes 6291458 | tf_op jit(solution)/shard_map/reduce_sum | solution.py:19
  193.6 3.2 copy.36
  196.8 16.3 %all-to-all-start.2 = ((bf16[64,2,8,1024]{3,2,1,0:T(8,128)(2,1)}), bf16[64,2,8,1024]{3,2,1,0:T(8,128)(2,1)}, u32[]{:S(2)}, u32[]{:S(2)}) async-start(bf16[64,2,8,1024]{3,2,1,0:T(8,128)(2,1)} %copy.36), calls=%async_computation.2 | async-start | bytes 4194304 | tf_op jit(solution)/shard_map/all_to_all | solution.py:71
  213.1 0.1 copy.37
  213.2 95.1 %all-to-all-done.2 = bf16[64,2,8,1024]{3,2,1,0:T(8,128)(2,1)} async-done(((bf16[64,2,8,1024]{3,2,1,0:T(8,128)(2,1)}), bf16[64,2,8,1024]{3,2,1,0:T(8,128)(2,1)}, u32[]{:S(2)}, u32[]{:S(2)}) %all-to-all-start.2) | async-done | bytes 2097184 | tf_op jit(solution)/shard_map/all_to_all | solution.py:71
  308.3 4.6 %gather_fusion.1 = bf16[512,1024]{1,0:T(8,128)(2,1)S(1)} fusion(bf16[1024,1024]{1,0:T(8,128)(2,1)} %bitcast.17, s32[1024]{0:T(1024)S(1)} %pad_clamp_fusion), kind=kCustom, calls=%fused_computation.1 | custom fusion | bytes 2099200 | tf_op jit(solution)/shard_map/gather | solution.py:74
  312.9 1.7 reshape.83
  314.6 3.0 multiply_reduce_fusion
  317.6 0.1 multiply_reduce_fusion.2
  317.7 6.1 %all-gather.1 = f32[2,1,128]{2,1,0:T(1,128)S(1)} all-gather(f32[1,1,128]{2,1,0:T(1,128)S(1)} %bitcast.70), channel_id=2, replica_groups=mesh['grp'=2,'ep'=64,'tp'=2] {'tp'}, dimensions={0}, use_global_device_ids=true | all-gather | bytes 1536 | tf_op jit(solution)/shard_map/all_gather | solution.py:23
  323.9 0.8 multiply_convert_fusion
  (29 shorter events, 0.3 us)
Async XLA Ops:
  6.5 164.0 %copy-start = (bf16[2,256,2048]{2,1,0:T(8,128)(2,1)S(1)}, bf16[2,256,2048]{2,1,0:T(8,128)(2,1)}, u32[]{:S(2)}) copy-start(bf16[2,256,2048]{2,1,0:T(8,128)(2,1)} %param.14) | copy-start | bytes 6291460
  6.6 2.5 copy-start.1
  6.6 159.8 %all-gather.4.cloned.1.call-start = ((), (), s32[]{:S(2)}) async-start(), calls=%async_computation.3 | async-start | bytes 6291456 | tf_op jit(solution)/shard_map/all_gather | solution.py:65
  6.6 6.4 %copy-start.4 = (f32[2048]{0:T(1024)S(1)}, f32[2048]{0:T(1024)}, u32[]{:S(2)}) copy-start(f32[2048]{0:T(1024)} %param.9) | copy-start | bytes 24580
  196.8 16.3 %copy-start.3 = (f32[128,4]{0,1:T(4,128)S(1)}, f32[128,4]{0,1:T(4,128)}, u32[]{:S(2)}) copy-start(f32[128,4]{0,1:T(4,128)} %param.11) | copy-start | bytes 6148
  196.8 111.5 %all-to-all-start.2 = ((bf16[64,2,8,1024]{3,2,1,0:T(8,128)(2,1)}), bf16[64,2,8,1024]{3,2,1,0:T(8,128)(2,1)}, u32[]{:S(2)}, u32[]{:S(2)}) async-start(bf16[64,2,8,1024]{3,2,1,0:T(8,128)(2,1)} %copy.36), calls=%async_computation.2 | async-start | bytes 4194304 | tf_op jit(solution)/shard_map/all_to_all | solution.py:71
  314.6 9.2 %copy-start.2 = (f32[1024]{0:T(1024)S(1)}, f32[1024]{0:T(1024)}, u32[]{:S(2)}) copy-start(f32[1024]{0:T(1024)} %param.15) | copy-start | bytes 12292
Sparse Core Ops, SparseCore 0:
  146.6 19.7 all-gather.3
where the time goes:
time: 332 us
  blocking collectives  139 us (42%)
  waiting for transfers between devices  115 us (35%)
  local copies, waits for them, and re-layouts  22.4 us (7%)
  starting transfers between devices  16.3 us (5%)
  other arithmetic  14.1 us (4%)
  between operations  13.6 us (4%)
  matrix products  11.3 us (3%)
    all_to_all x1, blocking collectives, body(): lax.all_to_all(sendbuf, 'ep', split_axis=0, concat_axis=0, tiled=True)  125 us
    all_to_all x1, waiting for transfers between devices, body(): lax.all_to_all(results, 'ep', split_axis=0, concat_axis=0, tiled=True)  95.1 us
    all_gather x1, waiting for transfers between devices, body(): arrived = lax.all_gather(arrived, 'tp', axis=3, tiled=True)  19.9 us
    all_to_all x1, starting transfers between devices, body(): lax.all_to_all(results, 'ep', split_axis=0, concat_axis=0, tiled=True)  16.3 us
    all_to_all x1, blocking collectives, sent_and_summed(): lax.all_to_all(tiles, axis, split_axis=0, concat_axis=0, tiled=True)  8.04 us
    dot_general x1, matrix products, body(): jnp.einsum('secf,efd->secd', hidden, w_down, preferred_element_type=jnp.f...  7.24 us
  transfers between devices with their start and end apart: 2, of which 2 were waited for; matrix products, arithmetic and copies ran while one was open for 0% of the time, Pallas kernels for 0%

commit v1 on v0

--- a/solution.py
+++ b/solution.py
@@ -5,6 +5,14 @@
 
 GROUPS = 4
 EPS = 1e-06
+
+
+def tiled_gather(array, axis, dim):
+    peers = lax.axis_size(axis)
+    repeats = [peers if d == dim else 1 for d in range(array.ndim)]
+    return lax.all_to_all(
+        jnp.tile(array, repeats), axis, split_axis=dim, concat_axis=dim, tiled=True
+    )
 
 
 def split_up(value, dim, peers):
@@ -62,7 +70,7 @@
         ep_count, local_experts, row_cap, half_width
     )
     arrived = lax.all_to_all(sendbuf, "ep", split_axis=0, concat_axis=0, tiled=True)
-    arrived = lax.all_gather(arrived, "tp", axis=3, tiled=True)
+    arrived = tiled_gather(arrived, "tp", 3)
     gate_act = jnp.einsum("secd,edf->secf", arrived, w_gate, preferred_element_type=jnp.float32)
     up_act = jnp.einsum("secd,edf->secf", arrived, w_up, preferred_element_type=jnp.float32)
     hidden = (jax.nn.silu(gate_act) * up_act).astype(jnp.bfloat16)

time: 332 us -> 351 us (1.057)
  local copies, waits for them, and re-layouts: 22.4 us -> 67.3 us
  waiting for transfers between devices: 115 us -> 94.9 us
  blocking collectives: 139 us -> 155 us
  between operations: 13.6 us -> 0.21 us
  starting transfers between devices: 16.3 us -> 7.55 us
    all_gather x1 -> x0, waiting for transfers between devices: 19.9 us -> none  [body(): arrived = lax.all_gather(arrived, 'tp', axis=3, tiled=True)]
    unnamed x13 -> x15, local copies, waits for them, and re-layouts: 0.25 us -> 20 us
    all_to_all x0 -> x1, blocking collectives: none -> 16.1 us  [tiled_gather(): lax.all_to_all(jnp.tile(array, repeats), axis, split_axis=dim, concat_axi...]
    all_to_all x0 -> x1, local copies, waits for them, and re-layouts: none -> 12 us  [tiled_gather(): lax.all_to_all(jnp.tile(array, repeats), axis, split_axis=dim, concat_axi...]
    all_to_all x1, starting transfers between devices: 16.3 us -> 7.55 us  [body(): lax.all_to_all(results, 'ep', split_axis=0, concat_axis=0, tiled=True)]
    all_to_all x1, local copies, waits for them, and re-layouts: 1.52 us -> 8.17 us  [body(): lax.all_to_all(sendbuf, 'ep', split_axis=0, concat_axis=0, tiled=True)]
    another operation x3 -> x4, local copies, waits for them, and re-layouts: 0.03 us -> 6.51 us  [the longest x1 6.49 us: tiled_gather(): jnp.tile(array, repeats)]
  transfers between devices with their start and end apart: 2 -> 1, of which waited for: 2 -> 1; matrix products, arithmetic and copies ran while one was open for 0% -> 0% of each run, Pallas kernels for 0% -> 0%
where the time goes in v1:
time: 351 us; the launch traced here: 350 us
  blocking collectives  155 us (44%)
  waiting for transfers between devices  94.9 us (27%)
  local copies, waits for them, and re-layouts  67.3 us (19%)
  other arithmetic  14.1 us (4%)
  matrix products  11.3 us (3%)
  starting transfers between devices  7.55 us (2%)
    all_to_all x1, blocking collectives, body(): lax.all_to_all(sendbuf, 'ep', split_axis=0, concat_axis=0, tiled=True)  125 us
    all_to_all x1, waiting for transfers between devices, body(): lax.all_to_all(results, 'ep', split_axis=0, concat_axis=0, tiled=True)  94.9 us
    unnamed x15, local copies, waits for them, and re-layouts  20 us
    all_to_all x1, blocking collectives, tiled_gather(): lax.all_to_all(jnp.tile(array, repeats), axis, split_axis=dim, concat_axi...  16.1 us
    all_to_all x1, local copies, waits for them, and re-layouts, tiled_gather(): lax.all_to_all(jnp.tile(array, repeats), axis, split_axis=dim, concat_axi...  12 us
    all_to_all x1, local copies, waits for them, and re-layouts, body(): lax.all_to_all(sendbuf, 'ep', split_axis=0, concat_axis=0, tiled=True)  8.17 us
    all_to_all x1, blocking collectives, sent_and_summed(): lax.all_to_all(tiles, axis, split_axis=0, concat_axis=0, tiled=True)  8.12 us
    all_to_all x1, starting transfers between devices, body(): lax.all_to_all(results, 'ep', split_axis=0, concat_axis=0, tiled=True)  7.55 us
  transfers between devices with their start and end apart: 1, of which 1 were waited for; matrix products, arithmetic and copies ran while one was open for 0% of the time, Pallas kernels for 0%

profile of v1, /device:TPU:33, one launch (start us, length us, event | category | flops | bytes accessed | tf_op | source)
XLA Modules:
  0.0 350.4 jit_solution(2604830941224924054)
XLA Ops:
  0.0 1.3 convert_element_type.36
  1.3 1.2 multiply_reduce_fusion.1
  2.5 0.1 copy.31
  2.9 0.1 copy.33
  3.0 0.2 fusion.24
  3.3 0.1 copy.30
  3.5 0.2 fusion.23
  3.8 2.4 scatter_custom_fusion
  6.3 0.1 broadcast_in_dim.16
  6.6 5.4 %gather_fusion = bf16[1024,1024]{1,0:T(8,128)(2,1)} fusion(bf16[128,1024]{1,0:T(8,128)(2,1)S(1)} %fusion.20, s32[1024]{0:T(1024)S(1)} %maximum_clamp_fusion), kind=kCustom, calls=%fused_computation | custom fusion | bytes 4198400 | tf_op jit(solution)/shard_map/gather | solution.py:46
  11.9 1.8 broadcast_select_fusion
  13.7 124.7 %all_to_all.20 = bf16[64,2,8,1024]{3,2,1,0:T(8,128)(2,1)} all-to-all(bf16[64,2,8,1024]{3,2,1,0:T(8,128)(2,1)S(1)} %broadcast_select_fusion), channel_id=1, replica_groups=mesh['grp'=2,'ep'=64,'tp'=2] {'ep'}, dimensions={0} | all-to-all | bytes 4194304 | tf_op jit(solution)/shard_map/all_to_all | solution.py:72
  138.4 8.2 %copy.35 = bf16[64,2,8,1024]{0,2,1,3:T(8,128)(2,1)} copy(bf16[64,2,8,1024]{3,2,1,0:T(8,128)(2,1)} %all_to_all.20) | data formatting | bytes 4194304 | tf_op jit(solution)/shard_map/all_to_all | solution.py:72
  146.6 6.5 %tile.4 = bf16[64,2,8,2,1024]{0,2,1,4,3:T(8,128)(2,1)} broadcast(bf16[64,2,8,1024]{0,2,1,3:T(8,128)(2,1)} %copy.35), dimensions={0,1,2,4} | broadcast | bytes 6291456 | tf_op jit(solution)/shard_map/tile | solution.py:14
  153.1 10.0 %reshape.122 = bf16[2,2,524288]{2,1,0:T(2,128)(2,1)} reshape(bf16[2048,2,8,64]{3,2,1,0:T(8,128)(2,1)} %bitcast.64) | data formatting | bytes 8388608
  163.1 16.1 %all_to_all.21 = bf16[2,2,524288]{2,1,0:T(2,128)(2,1)} all-to-all(bf16[2,2,524288]{2,1,0:T(2,128)(2,1)} %reshape.122), channel_id=1, replica_groups=mesh['grp'=2,'ep'=64,'tp'=2] {'tp'}, dimensions={0} | all-to-all | bytes 8388608 | tf_op jit(solution)/shard_map/all_to_all | solution.py:13
  179.2 9.8 %reshape.123 = bf16[2048,2,8,64]{3,2,1,0:T(8,128)(2,1)} reshape(bf16[2,2,524288]{2,1,0:T(2,128)(2,1)} %all_to_all.21) | data formatting | bytes 8388608
  189.0 12.0 %copy.36 = bf16[64,2,8,2048]{3,2,0,1:T(8,128)(2,1)} copy(bf16[64,2,8,2048]{0,2,1,3:T(8,128)(2,1)} %bitcast.65) | data formatting | bytes 8388608 | tf_op jit(solution)/shard_map/all_to_all | solution.py:13
  201.0 4.1 %fusion.5 = f32[64,2,8,256]{3,2,0,1:T(8,128)S(1)} fusion(bf16[64,2,8,2048]{3,2,0,1:T(8,128)(2,1)} %copy.36, bf16[2,2048,256]{2,1,0:T(8,128)(2,1)} %param.12), kind=kOutput, calls=%fused_computation.12 | convolution fusion | flops 1073741824 | bytes 7340032 | tf_op jit(solution)/shard_map/secd,edf->secf/dot_general | solution.py:74
  205.1 7.2 %convolution_convert_fusion = bf16[2,64,8,2048]{3,2,1,0:T(8,128)(2,1)} fusion(bf16[2,256,2048]{2,1,0:T(8,128)(2,1)S(1)} %copy-done, bf16[64,2,8,2048]{3,2,0,1:T(8,128)(2,1)} %copy.36, bf16[2,2048,256]{2,1,0:T(8,128)(2,1)} %param.13, f32[64,2,8,256]{3,2,0,1:T(8,128)S(1)} %fusion.5), kind=kOutput, calls=%fused_computation.4 | convolution fusion | flops 2151153664 | bytes 13631488 | tf_op jit(solution)/shard_map/secf,efd->secd/dot_general | solution.py:77
  212.3 2.6 copy.47
  214.9 8.1 %all_to_all.22 = bf16[2,64,2,8,1024]{4,3,1,2,0:T(8,128)(2,1)} all-to-all(bf16[2,64,2,8,1024]{4,3,1,2,0:T(8,128)(2,1)S(1)} %bitcast.66), channel_id=1, replica_groups=mesh['grp'=2,'ep'=64,'tp'=2] {'tp'}, dimensions={0} | all-to-all | bytes 8388608 | tf_op jit(solution)/shard_map/all_to_all | solution.py:26
  223.1 5.2 %reduce_sum.62 = bf16[64,2,8,1024]{3,2,0,1:T(8,128)(2,1)} reduce(bf16[2,64,2,8,1024]{4,3,1,2,0:T(8,128)(2,1)} %all_to_all.22, bf16[]{:T(256)} %constant.55.clone.1), dimensions={0}, to_apply=%region_5.6 | reduce | flops 1048576 | bytes 6291458 | tf_op jit(solution)/shard_map/reduce_sum | solution.py:27
  228.2 3.2 copy.40
  231.4 7.5 %all-to-all-start.3 = ((bf16[64,2,8,1024]{3,2,1,0:T(8,128)(2,1)}), bf16[64,2,8,1024]{3,2,1,0:T(8,128)(2,1)}, u32[]{:S(2)}, u32[]{:S(2)}) async-start(bf16[64,2,8,1024]{3,2,1,0:T(8,128)(2,1)} %copy.40), calls=%async_computation.3 | async-start | bytes 4194304 | tf_op jit(solution)/shard_map/all_to_all | solution.py:79
  239.1 94.9 %all-to-all-done.3 = bf16[64,2,8,1024]{3,2,1,0:T(8,128)(2,1)} async-done(((bf16[64,2,8,1024]{3,2,1,0:T(8,128)(2,1)}), bf16[64,2,8,1024]{3,2,1,0:T(8,128)(2,1)}, u32[]{:S(2)}, u32[]{:S(2)}) %all-to-all-start.3) | async-done | bytes 2097184 | tf_op jit(solution)/shard_map/all_to_all | solution.py:79
  334.0 4.6 %gather_fusion.1 = bf16[512,1024]{1,0:T(8,128)(2,1)S(1)} fusion(bf16[1024,1024]{1,0:T(8,128)(2,1)} %bitcast.18, s32[1024]{0:T(1024)S(1)} %pad_clamp_fusion), kind=kCustom, calls=%fused_computation.1 | custom fusion | bytes 2099200 | tf_op jit(solution)/shard_map/gather | solution.py:82
  338.6 1.7 reshape.87
  340.3 3.0 multiply_reduce_fusion
  343.3 0.1 multiply_reduce_fusion.2
  343.4 6.1 %all-gather.1 = f32[2,1,128]{2,1,0:T(1,128)S(1)} all-gather(f32[1,1,128]{2,1,0:T(1,128)S(1)} %bitcast.75), channel_id=2, replica_groups=mesh['grp'=2,'ep'=64,'tp'=2] {'tp'}, dimensions={0}, use_global_device_ids=true | all-gather | bytes 1536 | tf_op jit(solution)/shard_map/all_gather | solution.py:31
  349.5 0.8 multiply_convert_fusion
  (31 shorter events, 0.7 us)
Async XLA Ops:
  0.0 205.1 %copy-start = (bf16[2,256,2048]{2,1,0:T(8,128)(2,1)S(1)}, bf16[2,256,2048]{2,1,0:T(8,128)(2,1)}, u32[]{:S(2)}) copy-start(bf16[2,256,2048]{2,1,0:T(8,128)(2,1)} %param.14) | copy-start | bytes 6291460
  0.0 2.5 copy-start.1
  0.0 6.4 %copy-start.4 = (f32[2048]{0:T(1024)S(1)}, f32[2048]{0:T(1024)}, u32[]{:S(2)}) copy-start(f32[2048]{0:T(1024)} %param.9) | copy-start | bytes 24580
  231.4 7.6 %copy-start.3 = (f32[128,4]{0,1:T(4,128)S(1)}, f32[128,4]{0,1:T(4,128)}, u32[]{:S(2)}) copy-start(f32[128,4]{0,1:T(4,128)} %param.11) | copy-start | bytes 6148
  231.4 102.6 %all-to-all-start.3 = ((bf16[64,2,8,1024]{3,2,1,0:T(8,128)(2,1)}), bf16[64,2,8,1024]{3,2,1,0:T(8,128)(2,1)}, u32[]{:S(2)}, u32[]{:S(2)}) async-start(bf16[64,2,8,1024]{3,2,1,0:T(8,128)(2,1)} %copy.40), calls=%async_computation.3 | async-start | bytes 4194304 | tf_op jit(solution)/shard_map/all_to_all | solution.py:79
  340.3 9.2 %copy-start.2 = (f32[1024]{0:T(1024)S(1)}, f32[1024]{0:T(1024)}, u32[]{:S(2)}) copy-start(f32[1024]{0:T(1024)} %param.15) | copy-start | bytes 12292
